TPU v7x, 32 devices: a whole 2x2x4 slice. The times are simulated.
32 devices in a mesh: fs: 4 (over z), tp: 8 (over y, x, core).
Axes of the slice: x: 2, y: 2, z: 4, core: 2. Of those that a mesh axis runs over, the one named last changes fastest.
Arguments:
- tokens: bfloat16 [1024, 1344], P('fs'), may hold values from -6 to 6
- cotangent: bfloat16 [1024, 1344], P('fs'), may hold values from -8 to 8
- gate_weight: bfloat16 [1344, 3072], P('fs', 'tp'), may hold values from -0.15625 to 0.15625
- up_weight: bfloat16 [1344, 3072], P('fs', 'tp'), may hold values from -0.15625 to 0.15625
- down_weight: bfloat16 [3072, 1344], P('tp', 'fs'), may hold values from -0.109375 to 0.109375
Outputs:
- input_grad: bfloat16 [1024, 1344], P('fs')
- down_grad: float32 [3072, 1344], P('tp', 'fs')
All inputs are finite; a program needn't handle non-finite values.
Results may differ from a plain program's by a relative error of at most 0.013.
Values may be sent and summed in bfloat16 or wider, within the bound.
A program may use at most 64 MiB of HBM per device.

v0:
```python
import jax
import jax.numpy as jnp
from jax import lax
from jax.sharding import PartitionSpec as P


def contract_rows(left, right):
    return lax.dot_general(
        left, right, (((0,), (0,)), ((), ())), preferred_element_type=jnp.float32
    )


def contract_cols(left, right):
    return lax.dot_general(
        left, right, (((1,), (1,)), ((), ())), preferred_element_type=jnp.float32
    )


def send_down(hidden, cotangent):
    return lax.psum_scatter(
        contract_rows(cotangent, hidden), "fs", scatter_dimension=0, tiled=True
    ).T


def per_device(tokens, cotangent, gate_weight, up_weight, down_weight):
    whole_gate, whole_up, whole_down = (
        lax.all_gather(gate_weight, "fs", axis=0, tiled=True),
        lax.all_gather(up_weight, "fs", axis=0, tiled=True),
        lax.all_gather(down_weight, "fs", axis=1, tiled=True),
    )
    gate_pre = jnp.dot(tokens, whole_gate, preferred_element_type=jnp.float32)
    up_pre = jnp.dot(tokens, whole_up, preferred_element_type=jnp.float32)
    hidden_grad = contract_cols(cotangent, whole_down)
    sigmoid_gate = jax.nn.sigmoid(gate_pre)
    activated = gate_pre * sigmoid_gate
    hidden = (activated * up_pre).astype(jnp.bfloat16)
    gate_pre_grad = (
        hidden_grad * up_pre * sigmoid_gate * (1.0 + gate_pre * (1.0 - sigmoid_gate))
    ).astype(jnp.bfloat16)
    up_pre_grad = (hidden_grad * activated).astype(jnp.bfloat16)
    partial_value = contract_cols(gate_pre_grad, whole_gate) + contract_cols(up_pre_grad, whole_up)
    input_grad = lax.psum(partial_value.astype(jnp.bfloat16), "tp")
    down_grad = send_down(hidden, cotangent)
    return (input_grad, down_grad)


def solution(mesh):
    placed = (P("fs", None), P("fs", None), P("fs", "tp"), P("fs", "tp"), P("tp", "fs"))
    return jax.shard_map(
        per_device,
        mesh=mesh,
        in_specs=placed,
        out_specs=(P("fs", None), P("tp", "fs")),
        check_vma=False,
    )
```

profile of v0, /device:TPU:1, one launch (start us, length us, event | category | flops | bytes accessed | tf_op | source)
XLA Modules:
  0.0 141.8 jit_solution(16917599836536708158)
XLA Ops:
  8.0 0.0 copy-start
  8.0 0.0 copy-start.1
  8.0 0.0 copy-start.3
  8.0 0.0 all-reduce.2.cloned.1.call-start
  8.1 21.1 %all_gather.11 = bf16[1344,384]{1,0:T(8,128)(2,1)S(1)} all-gather(bf16[336,384]{1,0:T(8,128)(2,1)} %param.7), channel_id=1, replica_groups=mesh['fs'=4,'tp'=8] {'fs'}, dimensions={0}, use_global_device_ids=true | all-gather | bytes 1290240 | tf_op jit(solution)/shard_map/all_gather | solution.py:27
  29.2 0.0 copy-done.1
  29.2 19.3 %all_gather.10 = bf16[1344,384]{1,0:T(8,128)(2,1)S(1)} all-gather(bf16[336,384]{1,0:T(8,128)(2,1)S(1)} %copy-done.1), channel_id=1, replica_groups=mesh['fs'=4,'tp'=8] {'fs'}, dimensions={0}, use_global_device_ids=true | all-gather | bytes 1290240 | tf_op jit(solution)/shard_map/all_gather | solution.py:28
  48.4 0.0 copy-done.3
  48.4 0.6 fusion.11
  49.0 0.0 copy-start.2
  49.0 0.6 fusion.10
  49.6 0.3 copy-done.2
  50.0 20.3 %all_gather.9 = bf16[384,1344]{0,1:T(8,128)(2,1)S(1)} all-gather(bf16[384,336]{0,1:T(8,128)(2,1)S(1)} %copy-done.2), channel_id=1, replica_groups=mesh['fs'=4,'tp'=8] {'fs'}, dimensions={1}, use_global_device_ids=true | all-gather | bytes 1290240 | tf_op jit(solution)/shard_map/all_gather | solution.py:29
  70.3 0.0 copy-done
  70.3 0.6 fusion.9
  70.9 0.6 fusion.2
  71.6 1.5 %fusion = bf16[256,1344]{0,1:T(8,128)(2,1)} fusion(f32[256,1344]{0,1:T(8,128)S(1)} %fusion.2, bf16[1344,384]{1,0:T(8,128)(2,1)S(1)} %all_gather.10, f32[256,384]{1,0:T(8,128)S(1)} %fusion.9, f32[256,384]{1,0:T(8,128)S(1)} %fusion.11), kind=kOutput, calls=%fused_computation.2 | convolution fusion | flops 265519104 | bytes 3883008 | tf_op jit(solution)/shard_map/dot_general | solution.py:14
  73.0 0.0 all-reduce.2.cloned.1.call-update
  73.1 0.0 reduce-scatter.2.cloned.1.call-start
  73.1 1.9 %convolution_bitcast_fusion = f32[1344,384]{1,0:T(8,128)} fusion(bf16[256,1344]{0,1:T(8,128)(2,1)S(1)} %copy-done, f32[256,384]{1,0:T(8,128)S(1)} %fusion.10, f32[256,384]{1,0:T(8,128)S(1)} %fusion.11), kind=kOutput, calls=%fused_computation | convolution fusion | flops 264830976 | bytes 3538944 | tf_op jit(solution)/shard_map/dot_general | solution.py:8
  75.1 0.0 reduce-scatter.2.cloned.1.call-update
  75.1 57.3 %all-reduce.2.cloned.1.call-done = bf16[256,1344]{0,1:T(8,128)(2,1)} async-done(((bf16[256,1344]{0,1:T(8,128)(2,1)}), bf16[256,1344]{0,1:T(8,128)(2,1)}) %all-reduce.2.cloned.1.call-update) | async-done | bytes 688144 | tf_op jit(solution)/shard_map/psum | solution.py:42
  132.4 0.0 reduce-scatter.2.cloned.1.call-done
  132.4 2.0 %copy.8 = bf16[256,1344]{0,1:T(8,128)(2,1)} copy(bf16[256,1344]{0,1:T(8,128)(2,1)} %all-reduce.2.cloned.1.call-done) | data formatting | bytes 1376256
Async XLA Ops:
  8.0 62.3 %copy-start = (bf16[256,1344]{0,1:T(8,128)(2,1)S(1)}, bf16[256,1344]{0,1:T(8,128)(2,1)}, u32[]{:S(2)}) copy-start(bf16[256,1344]{0,1:T(8,128)(2,1)} %param.6) | copy-start | bytes 2064388
  8.0 21.2 %copy-start.1 = (bf16[336,384]{1,0:T(8,128)(2,1)S(1)}, bf16[336,384]{1,0:T(8,128)(2,1)}, u32[]{:S(2)}) copy-start(bf16[336,384]{1,0:T(8,128)(2,1)} %param.8) | copy-start | bytes 774148
  8.0 40.4 %copy-start.3 = (bf16[256,1344]{0,1:T(8,128)(2,1)S(1)}, bf16[256,1344]{0,1:T(8,128)(2,1)}, u32[]{:S(2)}) copy-start(bf16[256,1344]{0,1:T(8,128)(2,1)} %param.5) | copy-start | bytes 2064388
  8.0 124.4 %all-reduce.2.cloned.1.call-start = ((), (), s32[]{:S(2)}) async-start(), calls=%async_computation.1 | async-start | bytes 1376256 | tf_op jit(solution)/shard_map/psum | solution.py:42
  49.0 1.0 copy-start.2
  73.1 59.3 %reduce-scatter.2.cloned.1.call-start = ((), (), s32[]{:S(2)}) async-start(), calls=%async_computation.2 | async-start | bytes 2580480 | tf_op jit(solution)/shard_map/reduce_scatter | solution.py:20
Sparse Core Ops, SparseCore 0:
  73.2 59.1 all-reduce.1
Sparse Core Ops, SparseCore 1:
  76.4 47.0 reduce-scatter.1
where the time goes:
time: 143 us; the launch traced here: 142 us
  blocking collectives  60.7 us (42%)
  waiting for transfers between devices  57.3 us (40%)
  between operations  15.5 us (11%)
  matrix products  5.84 us (4%)
  local copies, waits for them, and re-layouts  2.35 us (2%)
    psum x1, waiting for transfers between devices, per_device(): input_grad = lax.psum(partial_value.astype(jnp.bfloat16), 'tp')  57.3 us
    all_gather x1, blocking collectives, per_device(): lax.all_gather(gate_weight, 'fs', axis=0, tiled=True)  21.1 us
    all_gather x1, blocking collectives, per_device(): lax.all_gather(down_weight, 'fs', axis=1, tiled=True)  20.3 us
    all_gather x1, blocking collectives, per_device(): lax.all_gather(up_weight, 'fs', axis=0, tiled=True)  19.3 us
  transfers between devices with their start and end apart: 2, of which 1 were waited for; matrix products, arithmetic and copies ran while one was open for 1% of the time, Pallas kernels for 0%

commit v1 on v0

--- a/solution.py
+++ b/solution.py
@@ -1,7 +1,16 @@
+import functools
+
 import jax
 import jax.numpy as jnp
 from jax import lax
+from jax.experimental import pallas as pl
+from jax.experimental.pallas import tpu as pltpu
 from jax.sharding import PartitionSpec as P
+
+LANES = 128
+SUB = 16
+BF16 = jnp.bfloat16
+F32 = jnp.float32
 
 
 def contract_rows(left, right):
@@ -22,7 +31,7 @@
     ).T
 
 
-def per_device(tokens, cotangent, gate_weight, up_weight, down_weight):
+def per_device_plain(tokens, cotangent, gate_weight, up_weight, down_weight):
     whole_gate, whole_up, whole_down = (
         lax.all_gather(gate_weight, "fs", axis=0, tiled=True),
         lax.all_gather(up_weight, "fs", axis=0, tiled=True),
@@ -44,7 +53,282 @@
     return (input_grad, down_grad)
 
 
+def kernel(n, tok_ref, cot_ref, gate_ref, up_ref, down_ref, dx_out, dg_out,
+           wgu, wd, cot4, dxacc, part, rsr, rss, rx1, rx2, rx3, tx1, tx2, tx3, ybuf,
+           ag_send, ag_recv, rs_send, rs_recv, ar_send, ar_recv, loc_sem):
+    z = lax.axis_index("fs")
+    b = lax.axis_index("tp")
+    rows, depth = tok_ref.shape
+    shard, ff = gate_ref.shape
+    chunks = ff // LANES
+    core = lax.rem(b, 2)
+    m2 = 2 + 2 * core
+    m3 = 6 - m2
+    bit2 = lax.rem(b // m2, 2)
+    bit3 = lax.rem(b // m3, 2)
+    p1 = b + 1 - 2 * core
+    p2 = b + m2 * (1 - 2 * bit2)
+    p3 = b + m3 * (1 - 2 * bit3)
+    has_left = z > 0
+    has_right = z < n - 1
+
+    def z_id(step):
+        return {"fs": z + step}
+
+    barrier = pltpu.get_barrier_semaphore()
+    for partner in (p1, p2, p3):
+        pl.semaphore_signal(barrier, inc=1, device_id={"tp": partner},
+                            device_id_type=pl.DeviceIdType.MESH)
+    for step, there in ((-1, has_left), (1, has_right)):
+        @pl.when(there)
+        def _():
+            pl.semaphore_signal(barrier, inc=1, device_id=z_id(step),
+                                device_id_type=pl.DeviceIdType.MESH)
+    peers = 3 + lax.div(z + n - 1, n) + lax.div(2 * n - 2 - z, n)
+    pl.semaphore_wait(barrier, peers)
+
+    def slot(c, s, kind):
+        r = pl.ds(pl.multiple_of(s * shard, SUB), shard)
+        if kind == 0:
+            return wgu.at[r, pl.ds(2 * c * LANES, LANES)]
+        if kind == 1:
+            return wgu.at[r, pl.ds((2 * c + 1) * LANES, LANES)]
+        return wd.at[s, pl.ds(c * LANES, LANES), :]
+
+    def own(c, kind):
+        if kind == 0:
+            return gate_ref.at[:, pl.ds(c * LANES, LANES)]
+        if kind == 1:
+            return up_ref.at[:, pl.ds(c * LANES, LANES)]
+        return down_ref.at[pl.ds(c * LANES, LANES), :]
+
+    def ag_copy(src, c, s, kind, side):
+        step = 1 if side else -1
+        return pltpu.make_async_remote_copy(
+            src_ref=src, dst_ref=slot(c, s, kind),
+            send_sem=ag_send.at[side, c, s, kind], recv_sem=ag_recv.at[c, s, kind],
+            device_id=z_id(step), device_id_type=pl.DeviceIdType.MESH)
+
+    def send_own(c):
+        for side, there in ((0, has_left), (1, has_right)):
+            @pl.when(there)
+            def _():
+                for kind in range(3):
+                    ag_copy(own(c, kind), c, z, kind, side).start()
+
+    def gather(c):
+        for d in range(1, n):
+            for side in (0, 1):
+                s = z - d if side == 0 else z + d
+                here = (z >= d) if side == 0 else (z + d <= n - 1)
+                onward = has_right if side == 0 else has_left
+                @pl.when(here)
+                def _():
+                    for kind in range(3):
+                        src = slot(c, s, kind)
+                        ag_copy(src, c, s, kind, 1 - side).wait_recv()
+                        @pl.when(onward)
+                        def _():
+                            ag_copy(src, c, s, kind, 1 - side).start()
+
+    def local_copy(c, kind):
+        return pltpu.make_async_copy(own(c, kind), slot(c, z, kind), loc_sem.at[c, kind])
+
+    send_own(0)
+    for c in range(chunks):
+        for kind in range(3):
+            local_copy(c, kind).start()
+    for k in range(n):
+        cot4[k] = cot_ref[:, k * shard:(k + 1) * shard]
+
+    def rs_copy(c, k, side):
+        return pltpu.make_async_remote_copy(
+            src_ref=rss.at[side, c, k], dst_ref=rsr.at[side, c, k],
+            send_sem=rs_send.at[side, c, k], recv_sem=rs_recv.at[side, c, k],
+            device_id=z_id(1 if side else -1), device_id_type=pl.DeviceIdType.MESH)
+
+    def rs_targets(side):
+        return range(n - 1, 0, -1) if side else range(n - 1)
+
+    def rs_start(c):
+        for side, end in ((1, z == 0), (0, z == n - 1)):
+            @pl.when(end)
+            def _():
+                for k in rs_targets(side):
+                    rss[side, c, k] = part[c, k].astype(BF16)
+                    rs_copy(c, k, side).start()
+
+    def rs_mid(c):
+        for side, middle in ((1, has_left), (0, has_right)):
+            for k in rs_targets(side):
+                ahead = (k > z) if side else (k < z)
+                @pl.when(jnp.logical_and(middle, ahead))
+                def _():
+                    rs_copy(c, k, side).wait_recv()
+                    rss[side, c, k] = (part[c, k] + rsr[side, c, k].astype(F32)).astype(BF16)
+                    rs_copy(c, k, side).start()
+
+    def rs_final(c):
+        r = pl.ds(c * LANES, LANES)
+        dg_out[r, :] = part[c, z]
+        for side, there in ((1, has_left), (0, has_right)):
+            @pl.when(there)
+            def _():
+                rs_copy(c, z, side).wait_recv()
+                dg_out[r, :] += rsr[side, c, z].astype(F32)
+
+    def ar_copy(i, src, dst, partner):
+        return pltpu.make_async_remote_copy(
+            src_ref=src, dst_ref=dst, send_sem=ar_send.at[i], recv_sem=ar_recv.at[i],
+            device_id={"tp": partner}, device_id_type=pl.DeviceIdType.MESH)
+
+    half, quarter, eighth = rows // 2, rows // 4, rows // 8
+    lo1 = core * half
+    other1 = (1 - core) * half
+    lo2 = lo1 + bit2 * quarter
+    other2 = lo1 + (1 - bit2) * quarter
+    lo3 = lo2 + bit3 * eighth
+    other3 = lo2 + (1 - bit3) * eighth
+
+    def at(lo, size):
+        return pl.ds(pl.multiple_of(lo, SUB), size)
+
+    ar1 = ar_copy(0, tx1, rx1, p1)
+    ar2 = ar_copy(1, tx2, rx2, p2)
+    ar3 = ar_copy(2, tx3, rx3, p3)
+
+    for c in range(chunks):
+        gather(c)
+        if c + 1 < chunks:
+            send_own(c + 1)
+        for kind in range(3):
+            local_copy(c, kind).wait()
+        w = wgu[:, 2 * c * LANES:(2 * c + 2) * LANES]
+        pre = jnp.dot(tok_ref[...], w, preferred_element_type=F32)
+        hg = contract_cols(cot4[0], wd[0, c * LANES:(c + 1) * LANES, :])
+        for k in range(1, n):
+            hg += contract_cols(cot4[k], wd[k, c * LANES:(c + 1) * LANES, :])
+        gate_pre, up_pre = pre[:, :LANES], pre[:, LANES:]
+        sig = jax.nn.sigmoid(gate_pre)
+        act = gate_pre * sig
+        hidden = act * up_pre
+        dgu = jnp.concatenate(
+            [(hg * up_pre * sig * (1.0 + gate_pre * (1.0 - sig))).astype(BF16),
+             (hg * act).astype(BF16)], axis=1)
+        if c == 0:
+            dxacc[...] = contract_cols(dgu, w)
+        else:
+            dxacc[...] += contract_cols(dgu, w)
+        if c == chunks - 1:
+            tx1[...] = dxacc[at(other1, half), :].astype(BF16)
+            ar1.start()
+        hidden_t = hidden.T.astype(BF16)
+        for k in range(n):
+            part[c, k] = jnp.dot(hidden_t, cot4[k], preferred_element_type=F32)
+        rs_start(c)
+        if c > 0 and c < chunks - 1:
+            rs_mid(c - 1)
+
+    ar1.wait_recv()
+    tx2[...] = (dxacc[at(other2, quarter), :]
+                + rx1[at(other2 - lo1, quarter), :].astype(F32)).astype(BF16)
+    ar2.start()
+    dxacc[at(lo2, quarter), :] += rx1[at(lo2 - lo1, quarter), :].astype(F32)
+    ar2.wait_recv()
+    tx3[...] = (dxacc[at(other3, eighth), :]
+                + rx2[at(other3 - lo2, eighth), :].astype(F32)).astype(BF16)
+    ar3.start()
+    dxacc[at(lo3, eighth), :] += rx2[at(lo3 - lo2, eighth), :].astype(F32)
+    ar3.wait_recv()
+    ybuf[at(lo3, eighth), :] = (dxacc[at(lo3, eighth), :] + rx3[...].astype(F32)).astype(BF16)
+    backs = []
+    for i, lo, size, partner in ((3, lo3, eighth, p3), (4, lo2, quarter, p2), (5, lo1, half, p1)):
+        own_rows = ybuf.at[at(lo, size), :]
+        back = ar_copy(i, own_rows, own_rows, partner)
+        back.start()
+        back.wait_recv()
+        backs.append(back)
+    dx_out[...] = ybuf[...]
+
+    for c in range(max(0, chunks - 2), chunks):
+        rs_mid(c)
+    for c in range(chunks):
+        rs_final(c)
+
+    for copy in [ar1, ar2, ar3] + backs:
+        copy.wait_send()
+    for side, there in ((0, has_left), (1, has_right)):
+        @pl.when(there)
+        def _():
+            for c in range(chunks):
+                for kind in range(3):
+                    ag_copy(own(c, kind), c, z, kind, side).wait_send()
+    for d in range(1, n):
+        for side in (0, 1):
+            s = z - d if side == 0 else z + d
+            here = (z >= d) if side == 0 else (z + d <= n - 1)
+            onward = has_right if side == 0 else has_left
+            @pl.when(jnp.logical_and(here, onward))
+            def _():
+                for c in range(chunks):
+                    for kind in range(3):
+                        ag_copy(slot(c, s, kind), c, s, kind, 1 - side).wait_send()
+    for side in (0, 1):
+        for k in rs_targets(side):
+            sent = (k > z) if side else (k < z)
+            @pl.when(sent)
+            def _():
+                for c in range(chunks):
+                    rs_copy(c, k, side).wait_send()
+
+
+def per_device_kernel(n, tokens, cotangent, gate_weight, up_weight, down_weight):
+    rows, depth = tokens.shape
+    shard, ff = gate_weight.shape
+    chunks = ff // LANES
+    vmem = pl.BlockSpec(memory_space=pltpu.VMEM)
+    dma = pltpu.SemaphoreType.DMA
+    return pl.pallas_call(
+        functools.partial(kernel, n),
+        out_shape=(jax.ShapeDtypeStruct((rows, depth), BF16),
+                   jax.ShapeDtypeStruct((ff, shard), F32)),
+        in_specs=[vmem] * 5,
+        out_specs=(vmem, vmem),
+        scratch_shapes=[
+            pltpu.VMEM((depth, 2 * ff), BF16),
+            pltpu.VMEM((n, ff, shard), BF16),
+            pltpu.VMEM((n, rows, shard), BF16),
+            pltpu.VMEM((rows, depth), F32),
+            pltpu.VMEM((chunks, n, LANES, shard), F32),
+            pltpu.VMEM((2, chunks, n, LANES, shard), BF16),
+            pltpu.VMEM((2, chunks, n, LANES, shard), BF16),
+            pltpu.VMEM((rows // 2, depth), BF16),
+            pltpu.VMEM((rows // 4, depth), BF16),
+            pltpu.VMEM((rows // 8, depth), BF16),
+            pltpu.VMEM((rows // 2, depth), BF16),
+            pltpu.VMEM((rows // 4, depth), BF16),
+            pltpu.VMEM((rows // 8, depth), BF16),
+            pltpu.VMEM((rows, depth), BF16),
+            dma((2, chunks, n, 3)), dma((chunks, n, 3)),
+            dma((2, chunks, n)), dma((2, chunks, n)),
+            dma((6,)), dma((6,)), dma((chunks, 3)),
+        ],
+        compiler_params=pltpu.CompilerParams(
+            collective_id=0, has_side_effects=True, vmem_limit_bytes=56 * 2**20),
+    )(tokens, cotangent, gate_weight, up_weight, down_weight)
+
+
 def solution(mesh):
+    n, tp = mesh.shape["fs"], mesh.shape["tp"]
+
+    def per_device(tokens, cotangent, gate_weight, up_weight, down_weight):
+        rows = tokens.shape[0]
+        shard, ff = gate_weight.shape
+        args = (tokens, cotangent, gate_weight, up_weight, down_weight)
+        fits = (tp == 8 and 2 <= n <= 8 and rows % (8 * SUB) == 0 and rows <= 512
+                and shard % SUB == 0 and ff % LANES == 0)
+        return per_device_kernel(n, *args) if fits else per_device_plain(*args)
+
     placed = (P("fs", None), P("fs", None), P("fs", "tp"), P("fs", "tp"), P("tp", "fs"))
     return jax.shard_map(
         per_device,

time: 143 us -> 104 us (0.73)
  Pallas kernels: 0 us -> 94.8 us
  blocking collectives: 60.7 us -> 0 us
  waiting for transfers between devices: 57.3 us -> 0 us
  between operations: 15.5 us -> 0.65 us
  local copies, waits for them, and re-layouts: 2.35 us -> 8.57 us
  matrix products: 5.84 us -> 0 us
    pallas_call x0 -> x1, Pallas kernels: none -> 94.8 us  [per_device_kernel(): pl.pallas_call(functools.partial(kernel, n), out_shape=(jax.ShapeDtypeStr...]
    all_gather x3 -> x0, blocking collectives: 60.7 us -> none  [the longest x1 21.1 us: per_device(): lax.all_gather(gate_weight, 'fs', axis=0, tiled=True)]
    psum x1 -> x0, waiting for transfers between devices: 57.3 us -> none  [per_device(): input_grad = lax.psum(partial_value.astype(jnp.bfloat16), 'tp')]
    dot_general x6 -> x0, matrix products: 5.84 us -> none  [the longest x3 2.71 us: contract_cols(): lax.dot_general(left, right, (((1,), (1,)), ((), ())), preferred_element_...]
    pallas_call x0 -> x2, local copies, waits for them, and re-layouts: none -> 3.28 us  [per_device_kernel(): pl.pallas_call(functools.partial(kernel, n), out_shape=(jax.ShapeDtypeStr...]
    unnamed x9 -> x7, local copies, waits for them, and re-layouts: 2.35 us -> 5.29 us
  transfers between devices with their start and end apart: 2 -> 0, of which waited for: 1 -> 0; matrix products, arithmetic and copies ran while one was open for 1% -> 0% of each run, Pallas kernels for 0% -> 0%
where the time goes in v1:
time: 104 us
  Pallas kernels  94.8 us (91%)
  local copies, waits for them, and re-layouts  8.57 us (8%)
    pallas_call x1, Pallas kernels, per_device_kernel(): pl.pallas_call(functools.partial(kernel, n), out_shape=(jax.ShapeDtypeStr...  94.8 us
    unnamed x7, local copies, waits for them, and re-layouts  5.29 us
    pallas_call x2, local copies, waits for them, and re-layouts, per_device_kernel(): pl.pallas_call(functools.partial(kernel, n), out_shape=(jax.ShapeDtypeStr...  3.28 us

profile of v1, /device:TPU:1, one launch (start us, length us, event | category | flops | bytes accessed | tf_op | source)
XLA Modules:
  0.0 104.0 jit_solution(2827537456879252743)
XLA Ops:
  0.6 1.8 %copy.9.down_ref = bf16[384,336]{1,0:T(8,128)(2,1)} copy(bf16[384,336]{0,1:T(8,128)(2,1)} %param.9) | data formatting | bytes 516096 | tf_op args[4]
  2.5 0.0 copy-start
  2.5 2.3 %copy.7.tok_ref = bf16[256,1344]{1,0:T(8,128)(2,1)} copy(bf16[256,1344]{0,1:T(8,128)(2,1)} %param.5) | data formatting | bytes 1376256 | tf_op args[0]
  4.8 0.0 copy-done
  4.8 1.2 %copy.8.cot_ref = bf16[256,1344]{1,0:T(8,128)(2,1)} copy(bf16[256,1344]{0,1:T(8,128)(2,1)S(1)} %copy-done) | data formatting | bytes 1376256 | tf_op args[1]
  5.9 94.8 %shard_map.68 = (bf16[256,1344]{1,0:T(8,128)(2,1)}, f32[384,336]{1,0:T(8,128)}) custom-call(bf16[256,1344]{1,0:T(8,128)(2,1)} %copy.7.tok_ref, bf16[256,1344]{1,0:T(8,128)(2,1)} %copy.8.cot_ref, bf16[336,384]{1,0:T(8,128)(2,1)} %gate_ref.1, bf16[336,384]{1,0:T(8,128)(2,1)} %up_ref.1, bf16[384,336]{1,0:T(8,128)(2,1)} %copy.9.down_ref), custom_call_target="tpu_custom_call" | custom-call | tf_op jit(solution)/shard_map/pallas_call | solution.py:291
  100.7 0.0 copy-start.1
  100.7 2.3 %copy.10 = bf16[256,1344]{0,1:T(8,128)(2,1)} copy(bf16[256,1344]{1,0:T(8,128)(2,1)} %get-tuple-element.2) | data formatting | bytes 1376256 | tf_op jit(solution)/shard_map/pallas_call | solution.py:291
  103.0 0.0 copy-done.1
  103.0 1.0 copy.11
Async XLA Ops:
  2.5 2.3 %copy-start = (bf16[256,1344]{0,1:T(8,128)(2,1)S(1)}, bf16[256,1344]{0,1:T(8,128)(2,1)}, u32[]{:S(2)}) copy-start(bf16[256,1344]{0,1:T(8,128)(2,1)} %param.6) | copy-start | bytes 2064388
  100.7 2.3 %copy-start.1 = (f32[384,336]{1,0:T(8,128)S(1)}, f32[384,336]{1,0:T(8,128)}, u32[]{:S(2)}) copy-start(f32[384,336]{1,0:T(8,128)} %get-tuple-element.3) | copy-start | bytes 1548292

commit v2 on v1

--- a/solution.py
+++ b/solution.py
@@ -134,7 +134,8 @@
     def local_copy(c, kind):
         return pltpu.make_async_copy(own(c, kind), slot(c, z, kind), loc_sem.at[c, kind])
 
-    send_own(0)
+    for c in range(min(2, chunks)):
+        send_own(c)
     for c in range(chunks):
         for kind in range(3):
             local_copy(c, kind).start()
@@ -199,8 +200,10 @@
 
     for c in range(chunks):
         gather(c)
-        if c + 1 < chunks:
-            send_own(c + 1)
+        if c + 2 < chunks:
+            send_own(c + 2)
+        if c >= 2:
+            rs_mid(c - 2)
         for kind in range(3):
             local_copy(c, kind).wait()
         w = wgu[:, 2 * c * LANES:(2 * c + 2) * LANES]
@@ -226,8 +229,6 @@
         for k in range(n):
             part[c, k] = jnp.dot(hidden_t, cot4[k], preferred_element_type=F32)
         rs_start(c)
-        if c > 0 and c < chunks - 1:
-            rs_mid(c - 1)
 
     ar1.wait_recv()
     tx2[...] = (dxacc[at(other2, quarter), :]

time: 104 us -> 100 us (0.962)
  Pallas kernels: 94.8 us -> 90.6 us
    pallas_call x1, Pallas kernels: 94.8 us -> 90.6 us  [per_device_kernel(): pl.pallas_call(functools.partial(kernel, n), out_shape=(jax.ShapeDtypeStr...]
where the time goes in v2:
time: 100 us; the launch traced here: 99.8 us
  Pallas kernels  90.6 us (91%)
  local copies, waits for them, and re-layouts  8.57 us (9%)
    pallas_call x1, Pallas kernels, per_device_kernel(): pl.pallas_call(functools.partial(kernel, n), out_shape=(jax.ShapeDtypeStr...  90.6 us
    unnamed x7, local copies, waits for them, and re-layouts  5.29 us
    pallas_call x2, local copies, waits for them, and re-layouts, per_device_kernel(): pl.pallas_call(functools.partial(kernel, n), out_shape=(jax.ShapeDtypeStr...  3.28 us

profile of v2, /device:TPU:1, one launch (start us, length us, event | category | flops | bytes accessed | tf_op | source)
XLA Modules:
  0.0 99.8 jit_solution(4883462805614786214)
XLA Ops:
  0.6 1.8 %copy.9.down_ref = bf16[384,336]{1,0:T(8,128)(2,1)} copy(bf16[384,336]{0,1:T(8,128)(2,1)} %param.9) | data formatting | bytes 516096 | tf_op args[4]
  2.5 0.0 copy-start
  2.5 2.3 %copy.7.tok_ref = bf16[256,1344]{1,0:T(8,128)(2,1)} copy(bf16[256,1344]{0,1:T(8,128)(2,1)} %param.5) | data formatting | bytes 1376256 | tf_op args[0]
  4.8 0.0 copy-done
  4.8 1.2 %copy.8.cot_ref = bf16[256,1344]{1,0:T(8,128)(2,1)} copy(bf16[256,1344]{0,1:T(8,128)(2,1)S(1)} %copy-done) | data formatting | bytes 1376256 | tf_op args[1]
  5.9 90.6 %shard_map.68 = (bf16[256,1344]{1,0:T(8,128)(2,1)}, f32[384,336]{1,0:T(8,128)}) custom-call(bf16[256,1344]{1,0:T(8,128)(2,1)} %copy.7.tok_ref, bf16[256,1344]{1,0:T(8,128)(2,1)} %copy.8.cot_ref, bf16[336,384]{1,0:T(8,128)(2,1)} %gate_ref.1, bf16[336,384]{1,0:T(8,128)(2,1)} %up_ref.1, bf16[384,336]{1,0:T(8,128)(2,1)} %copy.9.down_ref), custom_call_target="tpu_custom_call" | custom-call | tf_op jit(solution)/shard_map/pallas_call | solution.py:292
  96.5 0.0 copy-start.1
  96.5 2.3 %copy.10 = bf16[256,1344]{0,1:T(8,128)(2,1)} copy(bf16[256,1344]{1,0:T(8,128)(2,1)} %get-tuple-element.2) | data formatting | bytes 1376256 | tf_op jit(solution)/shard_map/pallas_call | solution.py:292
  98.8 0.0 copy-done.1
  98.8 1.0 %copy.11 = f32[384,336]{0,1:T(8,128)} copy(f32[384,336]{1,0:T(8,128)S(1)} %copy-done.1) | data formatting | bytes 1032192 | tf_op jit(solution)/shard_map/pallas_call | solution.py:292
Async XLA Ops:
  2.5 2.3 %copy-start = (bf16[256,1344]{0,1:T(8,128)(2,1)S(1)}, bf16[256,1344]{0,1:T(8,128)(2,1)}, u32[]{:S(2)}) copy-start(bf16[256,1344]{0,1:T(8,128)(2,1)} %param.6) | copy-start | bytes 2064388
  96.5 2.3 %copy-start.1 = (f32[384,336]{1,0:T(8,128)S(1)}, f32[384,336]{1,0:T(8,128)}, u32[]{:S(2)}) copy-start(f32[384,336]{1,0:T(8,128)} %get-tuple-element.3) | copy-start | bytes 1548292

commit v3 on v2

--- a/solution.py
+++ b/solution.py
@@ -54,11 +54,11 @@
 
 
 def kernel(n, tok_ref, cot_ref, gate_ref, up_ref, down_ref, dx_out, dg_out,
-           wgu, wd, cot4, dxacc, part, rsr, rss, rx1, rx2, rx3, tx1, tx2, tx3, ybuf,
+           weights, tok, cot, dxacc, part, rsr, rss, rx1, rx2, rx3, tx1, tx2, tx3, ybuf,
            ag_send, ag_recv, rs_send, rs_recv, ar_send, ar_recv, loc_sem):
     z = lax.axis_index("fs")
     b = lax.axis_index("tp")
-    rows, depth = tok_ref.shape
+    depth, rows = tok_ref.shape
     shard, ff = gate_ref.shape
     chunks = ff // LANES
     core = lax.rem(b, 2)
@@ -89,18 +89,10 @@
 
     def slot(c, s, kind):
         r = pl.ds(pl.multiple_of(s * shard, SUB), shard)
-        if kind == 0:
-            return wgu.at[r, pl.ds(2 * c * LANES, LANES)]
-        if kind == 1:
-            return wgu.at[r, pl.ds((2 * c + 1) * LANES, LANES)]
-        return wd.at[s, pl.ds(c * LANES, LANES), :]
+        return weights.at[r, pl.ds((3 * c + kind) * LANES, LANES)]
 
     def own(c, kind):
-        if kind == 0:
-            return gate_ref.at[:, pl.ds(c * LANES, LANES)]
-        if kind == 1:
-            return up_ref.at[:, pl.ds(c * LANES, LANES)]
-        return down_ref.at[pl.ds(c * LANES, LANES), :]
+        return (gate_ref, up_ref, down_ref)[kind].at[:, pl.ds(c * LANES, LANES)]
 
     def ag_copy(src, c, s, kind, side):
         step = 1 if side else -1
@@ -139,8 +131,8 @@
     for c in range(chunks):
         for kind in range(3):
             local_copy(c, kind).start()
-    for k in range(n):
-        cot4[k] = cot_ref[:, k * shard:(k + 1) * shard]
+    tok[...] = tok_ref[...].T
+    cot[...] = cot_ref[...].T
 
     def rs_copy(c, k, side):
         return pltpu.make_async_remote_copy(
@@ -171,25 +163,25 @@
 
     def rs_final(c):
         r = pl.ds(c * LANES, LANES)
-        dg_out[r, :] = part[c, z]
+        dg_out[:, r] = part[c, z]
         for side, there in ((1, has_left), (0, has_right)):
             @pl.when(there)
             def _():
                 rs_copy(c, z, side).wait_recv()
-                dg_out[r, :] += rsr[side, c, z].astype(F32)
+                dg_out[:, r] += rsr[side, c, z].astype(F32)
 
     def ar_copy(i, src, dst, partner):
         return pltpu.make_async_remote_copy(
             src_ref=src, dst_ref=dst, send_sem=ar_send.at[i], recv_sem=ar_recv.at[i],
             device_id={"tp": partner}, device_id_type=pl.DeviceIdType.MESH)
 
-    half, quarter, eighth = rows // 2, rows // 4, rows // 8
+    half, quarter, lanes = depth // 2, depth // 4, rows // 2
     lo1 = core * half
     other1 = (1 - core) * half
     lo2 = lo1 + bit2 * quarter
     other2 = lo1 + (1 - bit2) * quarter
-    lo3 = lo2 + bit3 * eighth
-    other3 = lo2 + (1 - bit3) * eighth
+    mine3 = pl.ds(pl.multiple_of(bit3 * lanes, LANES), lanes)
+    other3 = pl.ds(pl.multiple_of((1 - bit3) * lanes, LANES), lanes)
 
     def at(lo, size):
         return pl.ds(pl.multiple_of(lo, SUB), size)
@@ -206,28 +198,27 @@
             rs_mid(c - 2)
         for kind in range(3):
             local_copy(c, kind).wait()
-        w = wgu[:, 2 * c * LANES:(2 * c + 2) * LANES]
-        pre = jnp.dot(tok_ref[...], w, preferred_element_type=F32)
-        hg = contract_cols(cot4[0], wd[0, c * LANES:(c + 1) * LANES, :])
-        for k in range(1, n):
-            hg += contract_cols(cot4[k], wd[k, c * LANES:(c + 1) * LANES, :])
+        w = weights[:, 3 * c * LANES:(3 * c + 2) * LANES]
+        pre = jnp.dot(tok[...], w, preferred_element_type=F32)
+        hg = jnp.dot(cot[...], weights[:, (3 * c + 2) * LANES:(3 * c + 3) * LANES],
+                     preferred_element_type=F32)
         gate_pre, up_pre = pre[:, :LANES], pre[:, LANES:]
         sig = jax.nn.sigmoid(gate_pre)
         act = gate_pre * sig
-        hidden = act * up_pre
+        hidden = (act * up_pre).astype(BF16)
         dgu = jnp.concatenate(
             [(hg * up_pre * sig * (1.0 + gate_pre * (1.0 - sig))).astype(BF16),
              (hg * act).astype(BF16)], axis=1)
         if c == 0:
-            dxacc[...] = contract_cols(dgu, w)
+            dxacc[...] = contract_cols(w, dgu)
         else:
-            dxacc[...] += contract_cols(dgu, w)
+            dxacc[...] += contract_cols(w, dgu)
         if c == chunks - 1:
             tx1[...] = dxacc[at(other1, half), :].astype(BF16)
             ar1.start()
-        hidden_t = hidden.T.astype(BF16)
         for k in range(n):
-            part[c, k] = jnp.dot(hidden_t, cot4[k], preferred_element_type=F32)
+            part[c, k] = jnp.dot(cot_ref[k * shard:(k + 1) * shard, :], hidden,
+                                 preferred_element_type=F32)
         rs_start(c)
 
     ar1.wait_recv()
@@ -236,15 +227,16 @@
     ar2.start()
     dxacc[at(lo2, quarter), :] += rx1[at(lo2 - lo1, quarter), :].astype(F32)
     ar2.wait_recv()
-    tx3[...] = (dxacc[at(other3, eighth), :]
-                + rx2[at(other3 - lo2, eighth), :].astype(F32)).astype(BF16)
+    q = at(lo2, quarter)
+    tx3[...] = (dxacc[q, other3] + rx2[:, other3].astype(F32)).astype(BF16)
     ar3.start()
-    dxacc[at(lo3, eighth), :] += rx2[at(lo3 - lo2, eighth), :].astype(F32)
+    kept = dxacc[q, mine3] + rx2[:, mine3].astype(F32)
     ar3.wait_recv()
-    ybuf[at(lo3, eighth), :] = (dxacc[at(lo3, eighth), :] + rx3[...].astype(F32)).astype(BF16)
+    ybuf[q, mine3] = (kept + rx3[...].astype(F32)).astype(BF16)
     backs = []
-    for i, lo, size, partner in ((3, lo3, eighth, p3), (4, lo2, quarter, p2), (5, lo1, half, p1)):
-        own_rows = ybuf.at[at(lo, size), :]
+    whole = pl.ds(0, rows)
+    for i, r, l, partner in ((3, q, mine3, p3), (4, q, whole, p2), (5, at(lo1, half), whole, p1)):
+        own_rows = ybuf.at[r, l]
         back = ar_copy(i, own_rows, own_rows, partner)
         back.start()
         back.wait_recv()
@@ -289,34 +281,35 @@
     chunks = ff // LANES
     vmem = pl.BlockSpec(memory_space=pltpu.VMEM)
     dma = pltpu.SemaphoreType.DMA
-    return pl.pallas_call(
+    dx, dg = pl.pallas_call(
         functools.partial(kernel, n),
-        out_shape=(jax.ShapeDtypeStruct((rows, depth), BF16),
-                   jax.ShapeDtypeStruct((ff, shard), F32)),
+        out_shape=(jax.ShapeDtypeStruct((depth, rows), BF16),
+                   jax.ShapeDtypeStruct((shard, ff), F32)),
         in_specs=[vmem] * 5,
         out_specs=(vmem, vmem),
         scratch_shapes=[
-            pltpu.VMEM((depth, 2 * ff), BF16),
-            pltpu.VMEM((n, ff, shard), BF16),
-            pltpu.VMEM((n, rows, shard), BF16),
-            pltpu.VMEM((rows, depth), F32),
-            pltpu.VMEM((chunks, n, LANES, shard), F32),
-            pltpu.VMEM((2, chunks, n, LANES, shard), BF16),
-            pltpu.VMEM((2, chunks, n, LANES, shard), BF16),
-            pltpu.VMEM((rows // 2, depth), BF16),
-            pltpu.VMEM((rows // 4, depth), BF16),
-            pltpu.VMEM((rows // 8, depth), BF16),
-            pltpu.VMEM((rows // 2, depth), BF16),
-            pltpu.VMEM((rows // 4, depth), BF16),
-            pltpu.VMEM((rows // 8, depth), BF16),
+            pltpu.VMEM((depth, 3 * ff), BF16),
             pltpu.VMEM((rows, depth), BF16),
+            pltpu.VMEM((rows, depth), BF16),
+            pltpu.VMEM((depth, rows), F32),
+            pltpu.VMEM((chunks, n, shard, LANES), F32),
+            pltpu.VMEM((2, chunks, n, shard, LANES), BF16),
+            pltpu.VMEM((2, chunks, n, shard, LANES), BF16),
+            pltpu.VMEM((depth // 2, rows), BF16),
+            pltpu.VMEM((depth // 4, rows), BF16),
+            pltpu.VMEM((depth // 4, rows // 2), BF16),
+            pltpu.VMEM((depth // 2, rows), BF16),
+            pltpu.VMEM((depth // 4, rows), BF16),
+            pltpu.VMEM((depth // 4, rows // 2), BF16),
+            pltpu.VMEM((depth, rows), BF16),
             dma((2, chunks, n, 3)), dma((chunks, n, 3)),
             dma((2, chunks, n)), dma((2, chunks, n)),
             dma((6,)), dma((6,)), dma((chunks, 3)),
         ],
         compiler_params=pltpu.CompilerParams(
             collective_id=0, has_side_effects=True, vmem_limit_bytes=56 * 2**20),
-    )(tokens, cotangent, gate_weight, up_weight, down_weight)
+    )(tokens.T, cotangent.T, gate_weight, up_weight, down_weight.T)
+    return dx.T, dg.T
 
 
 def solution(mesh):
@@ -326,7 +319,7 @@
         rows = tokens.shape[0]
         shard, ff = gate_weight.shape
         args = (tokens, cotangent, gate_weight, up_weight, down_weight)
-        fits = (tp == 8 and 2 <= n <= 8 and rows % (8 * SUB) == 0 and rows <= 512
+        fits = (tp == 8 and 2 <= n <= 8 and rows % (2 * LANES) == 0 and tokens.shape[1] % (4 * SUB) == 0 and rows <= 512
                 and shard % SUB == 0 and ff % LANES == 0)
         return per_device_kernel(n, *args) if fits else per_device_plain(*args)
 

time: 100 us -> 91.3 us (0.913)
  local copies, waits for them, and re-layouts: 8.57 us -> 2.84 us
  Pallas kernels: 90.6 us -> 87.7 us
    pallas_call x2 -> x0, local copies, waits for them, and re-layouts: 3.28 us -> none  [per_device_kernel(): pl.pallas_call(functools.partial(kernel, n), out_shape=(jax.ShapeDtypeStr...]
    pallas_call x1, Pallas kernels: 90.6 us -> 87.7 us  [per_device_kernel(): pl.pallas_call(functools.partial(kernel, n), out_shape=(jax.ShapeDtypeStr...]
    unnamed x7 -> x4, local copies, waits for them, and re-layouts: 5.29 us -> 2.84 us
where the time goes in v3:
time: 91.3 us; the launch traced here: 91.1 us
  Pallas kernels  87.7 us (96%)
  local copies, waits for them, and re-layouts  2.84 us (3%)
    pallas_call x1, Pallas kernels, per_device_kernel(): pl.pallas_call(functools.partial(kernel, n), out_shape=(jax.ShapeDtypeStr...  87.7 us
    unnamed x4, local copies, waits for them, and re-layouts  2.84 us

profile of v3, /device:TPU:1, one launch (start us, length us, event | category | flops | bytes accessed | tf_op | source)
XLA Modules:
  0.0 91.1 jit_solution(9015037794264019529)
XLA Ops:
  0.6 87.7 %shard_map.68 = (bf16[1344,256]{1,0:T(8,128)(2,1)}, f32[336,384]{1,0:T(8,128)}) custom-call(bf16[1344,256]{1,0:T(8,128)(2,1)} %bitcast.5, bf16[1344,256]{1,0:T(8,128)(2,1)} %bitcast.6, bf16[336,384]{1,0:T(8,128)(2,1)} %gate_ref.1, bf16[336,384]{1,0:T(8,128)(2,1)} %up_ref.1, bf16[336,384]{1,0:T(8,128)(2,1)} %bitcast.9), custom_call_target="tpu_custom_call" | custom-call | tf_op jit(solution)/shard_map/pallas_call | solution.py:284
  88.3 0.0 copy-start
  88.3 2.0 %copy.9 = bf16[256,1344]{0,1:T(8,128)(2,1)} copy(bf16[256,1344]{0,1:T(8,128)(2,1)} %bitcast.7) | data formatting | bytes 1376256
  90.4 0.0 copy-done
  90.4 0.8 copy.10
Async XLA Ops:
  88.3 2.1 %copy-start = (f32[336,384]{1,0:T(8,128)S(1)}, f32[336,384]{1,0:T(8,128)}, u32[]{:S(2)}) copy-start(f32[336,384]{1,0:T(8,128)} %get-tuple-element.5) | copy-start | bytes 1548292
